TPU v7x, 32 devices: a whole 2x2x4 slice. The times are simulated.
32 devices in a mesh: sp: 4 (over z), tp: 8 (over y, x, core).
Axes of the slice: x: 2, y: 2, z: 4, core: 2. Of those that a mesh axis runs over, the one named last changes fastest.
Arguments:
- activations: bfloat16 [1024, 2048], P('sp', 'tp'), may hold values from -170 to 170
- norm_gain: float32 [2048], replicated, may hold values from 0.1 to 1.9
- query_weight: bfloat16 [2048, 1536], P(None, 'tp'), may hold values from -0.125 to 0.125
- latent_weight: bfloat16 [2048, 512], P(None, 'tp'), may hold values from -0.125 to 0.125
- rope_key_weight: bfloat16 [2048, 64], replicated, may hold values from -0.125 to 0.125
- latent_gain: float32 [512], replicated, may hold values from 1.5 to 64
- expand_weight: bfloat16 [512, 2048], P(None, 'tp'), may hold values from -0.25 to 0.25
- gate_weight: bfloat16 [2048, 1024], P(None, 'tp'), may hold values from -0.125 to 0.125
- pre_weight: bfloat16 [2048, 1024], P(None, 'tp'), may hold values from -0.125 to 0.125
- value_weight: bfloat16 [2048, 1024], P(None, 'tp'), may hold values from -0.125 to 0.125
- conv_kernel: bfloat16 [3, 1024], P(None, 'tp'), may hold values from -3.5 to 3.5
- output_attend: bfloat16 [1024, 2048], P('tp'), may hold values from -0.1875 to 0.1875
- output_conv: bfloat16 [1024, 2048], P('tp'), may hold values from -0.125 to 0.125
Outputs:
- mixed: bfloat16 [1024, 2048], P(('sp', 'tp'))
- log_weight_sum: float32 [8, 1024], P('tp', 'sp')
All inputs are finite; a program needn't handle non-finite values.
Results may differ from a plain program's by a relative error of at most 0.035.
The roundings to bfloat16 on the way count: a program that leaves them out, or rounds other values in their place, can miss the bound.
Values may be sent and summed in bfloat16 or wider, within the bound.
A program may use at most 128 MiB of HBM per device.

v0:
```python
import math
import jax
import jax.numpy as jnp
from jax import lax
from jax.sharding import PartitionSpec as P

D = 2048
NOPE = 128
ROPE = 64
VDIM = 128
GRID_W = 64
EPSILON = 1e-06
ROPE_BASE = 10000.0


def with_halo(array, sides, width):
    for axis, dim in sides:
        peers, length = (lax.axis_size(axis), array.shape[dim])
        up = [(i, (i + 1) % peers) for i in range(peers - 1)]
        down = [(j, i) for i, j in up]
        last = lax.slice_in_dim(array, length - width, length, axis=dim)
        leading = lax.slice_in_dim(array, 0, width, axis=dim)
        before = lax.ppermute(last, axis, up)
        after = lax.ppermute(leading, axis, down)
        array = jnp.concatenate([before, array, after], axis=dim)
    return array


def rotate(inputs, grid_rows, grid_cols):
    quarter = inputs.shape[-1] // 4
    inverse = ROPE_BASE ** (-jnp.arange(quarter, dtype=jnp.float32) / quarter)
    row_angle = (grid_rows[:, None] * inverse)[:, None, :]
    col_angle = (grid_cols[:, None] * inverse)[:, None, :]
    part_one = inputs[..., :quarter]
    part_two = inputs[..., quarter : 2 * quarter]
    part_three = inputs[..., 2 * quarter : 3 * quarter]
    part_four = inputs[..., 3 * quarter :]
    return jnp.concatenate(
        [
            part_one * jnp.cos(row_angle) - part_two * jnp.sin(row_angle),
            part_one * jnp.sin(row_angle) + part_two * jnp.cos(row_angle),
            part_three * jnp.cos(col_angle) - part_four * jnp.sin(col_angle),
            part_three * jnp.sin(col_angle) + part_four * jnp.cos(col_angle),
        ],
        axis=-1,
    )


def conv_branch(gate_proj, pre_proj, value_proj, conv_kernel):
    pre_mix = (pre_proj * value_proj).astype(jnp.bfloat16)
    padded = with_halo(pre_mix, (("sp", 0),), 1).astype(jnp.float32)
    kernel = conv_kernel.astype(jnp.float32)
    convolved = kernel[0] * padded[:-2] + kernel[1] * padded[1:-1] + kernel[2] * padded[2:]
    return (gate_proj * convolved).astype(jnp.bfloat16)


def body(
    activations,
    norm_gain,
    query_weight,
    latent_weight,
    rope_key_weight,
    latent_gain,
    expand_weight,
    gate_weight,
    pre_weight,
    value_weight,
    conv_kernel,
    output_attend,
    output_conv,
):
    tokens_here = activations.shape[0]
    query_cols = query_weight.shape[1]
    heads_here = query_cols // (NOPE + ROPE)
    latent_cols = latent_weight.shape[1]
    channels = gate_weight.shape[1]
    joined = jnp.concatenate(
        [query_weight, latent_weight, rope_key_weight, gate_weight, pre_weight, value_weight],
        axis=1,
    )
    inputs_f32 = activations.astype(jnp.float32)
    squares = lax.psum(jnp.sum(inputs_f32 * inputs_f32, axis=1, keepdims=True), "tp")
    partial_squares = jnp.zeros((tokens_here, 1), jnp.float32)
    piece_f32 = lax.all_gather(activations, "tp", axis=1, tiled=True).astype(jnp.float32)
    scaled = (piece_f32 * norm_gain).astype(jnp.bfloat16)
    running = jnp.dot(scaled, joined, preferred_element_type=jnp.float32)
    running, folded_squares = (running, partial_squares)
    inv_rms = lax.rsqrt(squares / D + EPSILON)
    projected = running * inv_rms
    latent_end = query_cols + latent_cols
    rope_end = latent_end + ROPE
    query_proj = projected[:, :query_cols]
    latent_proj = projected[:, query_cols:latent_end]
    rope_proj = projected[:, latent_end:rope_end]
    gate_proj = projected[:, rope_end : rope_end + channels]
    pre_proj = projected[:, rope_end + channels : rope_end + 2 * channels]
    value_proj = projected[:, rope_end + 2 * channels :]
    positions = lax.axis_index("sp") * tokens_here + jnp.arange(tokens_here, dtype=jnp.int32)
    grid_rows = (positions // GRID_W).astype(jnp.float32)
    grid_cols = (positions % GRID_W).astype(jnp.float32)
    query = query_proj.reshape(tokens_here, heads_here, NOPE + ROPE)
    query = jnp.concatenate(
        [query[..., :NOPE], rotate(query[..., NOPE:], grid_rows, grid_cols)], axis=-1
    )
    query = (query * (NOPE + ROPE) ** (-0.5)).astype(jnp.bfloat16)
    query_nope = query[..., :NOPE]
    query_rope = query[..., NOPE:]
    gathered = lax.all_gather(latent_proj.astype(jnp.bfloat16), "tp", axis=1, tiled=True).astype(
        jnp.float32
    )
    latent = (
        gathered
        * lax.rsqrt(jnp.mean(gathered * gathered, axis=1, keepdims=True) + EPSILON)
        * latent_gain
    ).astype(jnp.bfloat16)
    expanded = jnp.dot(latent, expand_weight, preferred_element_type=jnp.float32).astype(
        jnp.bfloat16
    )
    rope_key = rotate(rope_proj[:, None, :], grid_rows, grid_cols)[:, 0].astype(jnp.bfloat16)
    starting = (
        jnp.full((heads_here, tokens_here), -jnp.inf, jnp.float32),
        jnp.zeros((heads_here, tokens_here), jnp.float32),
        jnp.zeros((tokens_here, heads_here, VDIM), jnp.float32),
    )
    key_piece = lax.all_gather(expanded, "sp", axis=0, tiled=True)
    rope_piece = lax.all_gather(rope_key, "sp", axis=0, tiled=True)
    piece_rows = key_piece.shape[0]
    key_block = math.gcd(piece_rows, 1024)
    split_heads = key_piece.reshape(piece_rows, heads_here, NOPE + VDIM)

    def one_block(turn_index, state):
        row_max, row_sum, running_out = state
        offset = turn_index * key_block
        block_keys = lax.dynamic_slice_in_dim(split_heads, offset, key_block, 0)
        block_rope = lax.dynamic_slice_in_dim(rope_piece, offset, key_block, 0)
        scores = jnp.einsum(
            "thd,jhd->htj", query_nope, block_keys[..., :NOPE], preferred_element_type=jnp.float32
        )
        scores = scores + jnp.einsum(
            "thd,jd->htj", query_rope, block_rope, preferred_element_type=jnp.float32
        )
        new_max = jnp.maximum(row_max, jnp.max(scores, axis=-1))
        rescale = jnp.exp(row_max - new_max)
        weights = jnp.exp(scores - new_max[..., None])
        row_sum = row_sum * rescale + jnp.sum(weights, axis=-1)
        running_out = running_out * rescale.T[..., None] + jnp.einsum(
            "htj,jhd->thd",
            weights.astype(jnp.bfloat16),
            block_keys[..., NOPE:],
            preferred_element_type=jnp.float32,
        )
        return (new_max, row_sum, running_out)

    row_max, row_sum, running_out = lax.fori_loop(0, piece_rows // key_block, one_block, starting)
    attended = (
        (running_out / row_sum.T[..., None])
        .astype(jnp.bfloat16)
        .reshape(tokens_here, heads_here * VDIM)
    )
    log_weight_sum = row_max + jnp.log(row_sum)
    conv_mixed = conv_branch(gate_proj, pre_proj, value_proj, conv_kernel)
    mixed = lax.psum_scatter(
        (
            jnp.dot(attended, output_attend, preferred_element_type=jnp.float32)
            + jnp.dot(conv_mixed, output_conv, preferred_element_type=jnp.float32)
        ).astype(jnp.bfloat16),
        "tp",
        scatter_dimension=0,
        tiled=True,
    )
    return (mixed, log_weight_sum)


def solution(mesh):
    return jax.shard_map(
        body,
        mesh=mesh,
        in_specs=(
            P("sp", "tp"),
            P(),
            P(None, "tp"),
            P(None, "tp"),
            P(),
            P(),
            P(None, "tp"),
            P(None, "tp"),
            P(None, "tp"),
            P(None, "tp"),
            P(None, "tp"),
            P("tp", None),
            P("tp", None),
        ),
        out_specs=(P(("sp", "tp"), None), P("tp", "sp")),
        check_vma=False,
    )
```

profile of v0, /device:TPU:0, one launch (start us, length us, event | category | flops | bytes accessed | tf_op | source)
XLA Modules:
  0.0 135.6 jit_solution(17453811287171782455)
XLA Ops:
  7.3 0.7 all-gather.3.cloned.1.call-update
  8.0 1.0 multiply_reduce_fusion
  9.0 1.2 copy.19
  10.3 1.3 copy.20
  11.5 1.2 copy.21
  12.8 15.2 %psum.7 = f32[256,1]{0,1:T(1,128)S(1)} all-reduce(f32[256,1]{0,1:T(1,128)S(1)} %bitcast.73), channel_id=1, replica_groups=mesh['sp'=4,'tp'=8] {'tp'}, use_global_device_ids=true, to_apply=%region_1.0 | all-reduce | flops 256 | bytes 2048 | tf_op jit(solution)/shard_map/psum | solution.py:82
  28.0 0.6 slice_bitcast_fusion.13
  28.6 0.9 constant_dynamic-update-slice_fusion.5
  29.6 0.7 constant_dynamic-update-slice_fusion.4
  30.3 0.7 constant_dynamic-update-slice_fusion.3
  31.0 0.8 constant_dynamic-update-slice_fusion.2
  31.8 0.9 constant_dynamic-update-slice_fusion.1
  32.7 0.8 constant_dynamic-update-slice_fusion
  33.5 2.7 %all-gather.3.cloned.1.call-done = bf16[256,2048]{1,0:T(8,128)(2,1)} async-done(((bf16[256,256]{1,0:T(8,128)(2,1)}), bf16[256,2048]{1,0:T(8,128)(2,1)}) %all-gather.3.cloned.1.call-update) | async-done | bytes 1048592 | tf_op jit(solution)/shard_map/all_gather | solution.py:84
  36.2 3.1 %convolution_multiply_fusion = f32[256,704]{0,1:T(8,128)S(1)} fusion(bf16[2048,704]{0,1:T(8,128)(2,1)} %constant_dynamic-update-slice_fusion, bf16[256,2048]{1,0:T(8,128)(2,1)} %all-gather.3.cloned.1.call-done, f32[2048]{0:T(1024)S(1)} %copy-done.7, f32[256]{0:T(256)S(1)} %bitcast.74), kind=kOutput, calls=%fused_computation.6 | convolution fusion | flops 739950592 | bytes 4662272 | tf_op jit(solution)/shard_map/dot_general | solution.py:86
  39.4 0.1 constant_dynamic-update-slice_fusion.9
  39.6 0.1 constant_dynamic-update-slice_fusion.8
  39.7 0.2 fusion.52
  39.9 13.4 %all-gather = bf16[1024,1,64]{0,2,1:T(8,128)(2,1)S(1)} all-gather(bf16[256,1,64]{0,2,1:T(8,128)(2,1)S(1)} %pad_maximum_fusion), channel_id=2, replica_groups=mesh['sp'=4,'tp'=8] {'sp'}, dimensions={0}, use_global_device_ids=true | all-gather | bytes 163840 | tf_op jit(solution)/shard_map/all_gather | solution.py:126
  53.5 9.3 %all_gather.13 = bf16[256,512]{0,1:T(8,128)(2,1)S(1)} all-gather(bf16[256,64]{0,1:T(8,128)(2,1)S(1)} %slice.196), channel_id=1, replica_groups=mesh['sp'=4,'tp'=8] {'tp'}, dimensions={1}, use_global_device_ids=true | all-gather | bytes 294912 | tf_op jit(solution)/shard_map/all_gather | solution.py:108
  62.9 0.4 convolution_convert_fusion
  63.3 16.1 %all_gather.14 = bf16[1024,256]{1,0:T(8,128)(2,1)S(1)} all-gather(bf16[256,256]{1,0:T(8,128)(2,1)S(1)} %convolution_convert_fusion), channel_id=1, replica_groups=mesh['sp'=4,'tp'=8] {'sp'}, dimensions={0}, use_global_device_ids=true | all-gather | bytes 655360 | tf_op jit(solution)/shard_map/all_gather | solution.py:125
  79.4 0.3 convolution_bitcast_fusion.1
  79.7 0.4 fusion.66
  80.2 0.3 fusion.7
  80.5 3.7 %collective-permute-start = (bf16[1,128]{0,1:T(8,128)(2,1)S(1)}, bf16[1,128]{0,1:T(8,128)(2,1)S(1)}, u32[]{:S(2)}, u32[]{:S(2)}) collective-permute-start(bf16[1,128]{0,1:T(8,128)(2,1)S(1)} %get-tuple-element.26), channel_id=1, source_target_pairs={{0,8},{8,16},{16,24},{1,9},{9,17},{17,25},{2,10},{10,18},{18,26},{... | collective-permute-start | bytes 776 | tf_op jit(solution)/shard_map/ppermute | solution.py:23
  84.2 1.3 collective-permute-start.1
  85.5 2.4 %fusion.9 = f32[256,2048]{1,0:T(8,128)} fusion(bf16[128,2048]{1,0:T(8,128)(2,1)S(1)} %copy-done, f32[1,256,1024]{2,1,0:T(8,128)S(1)} %get-tuple-element.44, f32[256]{0:T(256)S(1)} %get-tuple-element.43, bf16[1024,1,256]{2,0,1:T(8,128)(2,1)S(1)} %bitcast.70, f32[256]{0:T(256)S(1)} %get-tuple-element.42, f32[256]{0:T(256)S(1)} %get-tuple-element.41), kind=kOutput, calls=%fused_computation.19 | convolution fusion | flops 201949184 | bytes 3935232 | tf_op jit(solution)/shard_map/dot_general | solution.py:164
  88.0 2.1 %collective-permute-done.1 = bf16[1,128]{0,1:T(8,128)(2,1)S(1)} collective-permute-done((bf16[1,128]{0,1:T(8,128)(2,1)S(1)}, bf16[1,128]{0,1:T(8,128)(2,1)S(1)}, u32[]{:S(2)}, u32[]{:S(2)}) %collective-permute-start.1) | collective-permute-done | bytes 288 | tf_op jit(solution)/shard_map/ppermute | solution.py:24
  90.2 3.2 %fusion = bf16[256,2048]{1,0:T(8,128)(2,1)} fusion(f32[256,2048]{1,0:T(8,128)} %fusion.9, bf16[128,2048]{1,0:T(8,128)(2,1)S(1)} %copy-done.2, f32[258,128]{0,1:T(8,128)S(1)} %maximum_convert_fusion, f32[256,704]{0,1:T(8,128)S(1)} %convolution_multiply_fusion, f32[128]{0:T(128)} %get-tuple-element.38, f32[128]{0:T(128)} %get-tuple-element.39, ...), kind=kOutput, calls=%fused_computation.1 | convolution fusion | flops 135495680 | bytes 4195840 | tf_op jit(solution)/shard_map/dot_general | solution.py:165
  93.4 0.6 log_add_fusion
  94.0 34.8 %reduce-scatter.2.cloned.1.call-done = bf16[32,2048]{1,0:T(8,128)(2,1)} async-done(((bf16[256,2048]{1,0:T(8,128)(2,1)}), bf16[32,2048]{1,0:T(8,128)(2,1)}) %reduce-scatter.2.cloned.1.call-update) | async-done | bytes 131088 | tf_op jit(solution)/shard_map/reduce_scatter | solution.py:162
  (39 shorter events, 0.7 us)
Async XLA Ops:
  7.2 78.4 %copy-start = (bf16[128,2048]{1,0:T(8,128)(2,1)S(1)}, bf16[128,2048]{1,0:T(8,128)(2,1)}, u32[]{:S(2)}) copy-start(bf16[128,2048]{1,0:T(8,128)(2,1)} %param.24) | copy-start | bytes 1572868
  7.2 20.8 %copy-start.5 = (bf16[3,128]{1,0:T(4,128)(2,1)S(1)}, bf16[3,128]{1,0:T(4,128)(2,1)}, u32[]{:S(2)}) copy-start(bf16[3,128]{1,0:T(4,128)(2,1)} %param.23) | copy-start | bytes 2308
  7.2 21.4 %copy-start.1 = (bf16[2048,192]{0,1:T(8,128)(2,1)S(1)}, bf16[2048,192]{0,1:T(8,128)(2,1)}, u32[]{:S(2)}) copy-start(bf16[2048,192]{0,1:T(8,128)(2,1)} %param.15) | copy-start | bytes 2359300
  7.2 22.3 %copy-start.3 = (bf16[2048,64]{0,1:T(8,128)(2,1)S(1)}, bf16[2048,64]{0,1:T(8,128)(2,1)}, u32[]{:S(2)}) copy-start(bf16[2048,64]{0,1:T(8,128)(2,1)} %param.16) | copy-start | bytes 786436
  7.2 23.1 %copy-start.4 = (bf16[2048,64]{0,1:T(8,128)(2,1)S(1)}, bf16[2048,64]{0,1:T(8,128)(2,1)}, u32[]{:S(2)}) copy-start(bf16[2048,64]{0,1:T(8,128)(2,1)} %param.17) | copy-start | bytes 786436
  7.2 29.0 %all-gather.3.cloned.1.call-start = ((), (), s32[]{:S(2)}) async-start(), calls=%async_computation.1 | async-start | bytes 1179648 | tf_op jit(solution)/shard_map/all_gather | solution.py:84
  8.0 120.8 %reduce-scatter.2.cloned.1.call-start = ((), (), s32[]{:S(2)}) async-start(), calls=%async_computation.2 | async-start | bytes 1179648 | tf_op jit(solution)/shard_map/reduce_scatter | solution.py:162
  28.6 7.6 %copy-start.7 = (f32[2048]{0:T(1024)S(1)}, f32[2048]{0:T(1024)}, u32[]{:S(2)}) copy-start(f32[2048]{0:T(1024)} %param.14) | copy-start | bytes 24580
  36.2 26.7 %copy-start.6 = (bf16[512,256]{1,0:T(8,128)(2,1)S(1)}, bf16[512,256]{1,0:T(8,128)(2,1)}, u32[]{:S(2)}) copy-start(bf16[512,256]{1,0:T(8,128)(2,1)} %param.19) | copy-start | bytes 786436
  36.2 26.7 %copy-start.8 = (f32[512]{0:T(512)S(1)}, f32[512]{0:T(512)}, u32[]{:S(2)}) copy-start(f32[512]{0:T(512)} %param.18) | copy-start | bytes 6148
  80.1 10.0 %copy-start.2 = (bf16[128,2048]{1,0:T(8,128)(2,1)S(1)}, bf16[128,2048]{1,0:T(8,128)(2,1)}, u32[]{:S(2)}) copy-start(bf16[128,2048]{1,0:T(8,128)(2,1)} %param.25) | copy-start | bytes 1572868
  80.5 7.4 %collective-permute-start = (bf16[1,128]{0,1:T(8,128)(2,1)S(1)}, bf16[1,128]{0,1:T(8,128)(2,1)S(1)}, u32[]{:S(2)}, u32[]{:S(2)}) collective-permute-start(bf16[1,128]{0,1:T(8,128)(2,1)S(1)} %get-tuple-element.26), channel_id=1, source_target_pairs={{0,8},{8,16},{16,24},{1,9},{9,17},{17,25},{2,10},{10,18},{18,26},{... | collective-permute-start | bytes 776 | tf_op jit(solution)/shard_map/ppermute | solution.py:23
  84.2 5.8 %collective-permute-start.1 = (bf16[1,128]{0,1:T(8,128)(2,1)S(1)}, bf16[1,128]{0,1:T(8,128)(2,1)S(1)}, u32[]{:S(2)}, u32[]{:S(2)}) collective-permute-start(bf16[1,128]{0,1:T(8,128)(2,1)S(1)} %get-tuple-element.36), channel_id=1, source_target_pairs={{8,0},{16,8},{24,16},{9,1},{17,9},{25,17},{10,2},{18,10},{26,18},{... | collective-permute-start | bytes 776 | tf_op jit(solution)/shard_map/ppermute | solution.py:24
Sparse Core Ops, SparseCore 0:
  9.9 26.2 all-gather.2
  93.5 35.1 reduce-scatter.1
where the time goes:
time: 136 us
  blocking collectives  53.9 us (40%)
  waiting for transfers between devices  40.2 us (30%)
  between operations  14.3 us (11%)
  matrix products  9.9 us (7%)
  local copies, waits for them, and re-layouts  9.39 us (7%)
  starting transfers between devices  5.04 us (4%)
  other arithmetic  2.83 us (2%)
    reduce_scatter x1, waiting for transfers between devices, body(): lax.psum_scatter((jnp.dot(attended, output_attend, preferred_element_type...  34.8 us
    all_gather x1, blocking collectives, body(): key_piece = lax.all_gather(expanded, 'sp', axis=0, tiled=True)  16.1 us
    psum x1, blocking collectives, body(): lax.psum(jnp.sum(inputs_f32 * inputs_f32, axis=1, keepdims=True), 'tp')  15.2 us
    all_gather x1, blocking collectives, body(): rope_piece = lax.all_gather(rope_key, 'sp', axis=0, tiled=True)  13.4 us
    all_gather x1, blocking collectives, body(): lax.all_gather(latent_proj.astype(jnp.bfloat16), 'tp', axis=1, tiled=True)  9.26 us
    unnamed x27, local copies, waits for them, and re-layouts  7.86 us
    ppermute x1, starting transfers between devices, with_halo(): before = lax.ppermute(last, axis, up)  3.67 us
    dot_general x1, matrix products, body(): jnp.dot(conv_mixed, output_conv, preferred_element_type=jnp.float32)  3.22 us
  transfers between devices with their start and end apart: 4, of which 3 were waited for; matrix products, arithmetic and copies ran while one was open for 10% of the time, Pallas kernels for 0%

commit v1 on v0

--- a/solution.py
+++ b/solution.py
@@ -11,6 +11,20 @@
 GRID_W = 64
 EPSILON = 1e-06
 ROPE_BASE = 10000.0
+
+
+def targets_tell(z):
+    n_parts = lax.axis_size("sp")
+    piece_next = z
+    next_value = [(idx - 1, idx) for idx in range(1, n_parts)] + [(n_parts - 1, 0)]
+    nth = 0
+    cards = [piece_next]
+    while nth < n_parts - 1:
+        piece_next = lax.ppermute(piece_next, axis_name="sp", perm=next_value)
+        cards += [piece_next]
+        nth = nth + 1
+    newest = jnp.concatenate([*reversed(cards)], 0)
+    return jnp.roll(newest, (lax.axis_index("sp") + 1) * piece_next.shape[0], 0)
 
 
 def with_halo(array, sides, width):
@@ -123,7 +137,7 @@
         jnp.zeros((tokens_here, heads_here, VDIM), jnp.float32),
     )
     key_piece = lax.all_gather(expanded, "sp", axis=0, tiled=True)
-    rope_piece = lax.all_gather(rope_key, "sp", axis=0, tiled=True)
+    rope_piece = targets_tell(rope_key)
     piece_rows = key_piece.shape[0]
     key_block = math.gcd(piece_rows, 1024)
     split_heads = key_piece.reshape(piece_rows, heads_here, NOPE + VDIM)

time: 136 us -> 131 us (0.963)
  blocking collectives: 53.9 us -> 40.2 us
  waiting for transfers between devices: 40.2 us -> 45.6 us
  starting transfers between devices: 5.04 us -> 8.32 us
    all_gather x1 -> x0, blocking collectives: 13.4 us -> none  [body(): rope_piece = lax.all_gather(rope_key, 'sp', axis=0, tiled=True)]
    ppermute x0 -> x3, waiting for transfers between devices: none -> 9.4 us  [targets_tell(): piece_next = lax.ppermute(piece_next, axis_name='sp', perm=next_value)]
    ppermute x0 -> x3, starting transfers between devices: none -> 4.24 us  [targets_tell(): piece_next = lax.ppermute(piece_next, axis_name='sp', perm=next_value)]
    ppermute x1, waiting for transfers between devices: 2.06 us -> 0.01 us  [with_halo(): after = lax.ppermute(leading, axis, down)]
    reduce_scatter x1, waiting for transfers between devices: 34.8 us -> 32.8 us  [body(): lax.psum_scatter((jnp.dot(attended, output_attend, preferred_element_type...]
    unnamed x27 -> x33, local copies, waits for them, and re-layouts: 7.86 us -> 7.88 us
  transfers between devices with their start and end apart: 4 -> 7, of which waited for: 3 -> 4; matrix products, arithmetic and copies ran while one was open for 10% -> 9% of each run, Pallas kernels for 0% -> 0%
where the time goes in v1:
time: 131 us
  waiting for transfers between devices  45.6 us (35%)
  blocking collectives  40.2 us (31%)
  between operations  14.4 us (11%)
  matrix products  9.9 us (8%)
  local copies, waits for them, and re-layouts  9.37 us (7%)
  starting transfers between devices  8.32 us (6%)
  other arithmetic  2.84 us (2%)
    reduce_scatter x1, waiting for transfers between devices, body(): lax.psum_scatter((jnp.dot(attended, output_attend, preferred_element_type...  32.8 us
    all_gather x1, blocking collectives, body(): key_piece = lax.all_gather(expanded, 'sp', axis=0, tiled=True)  15.8 us
    psum x1, blocking collectives, body(): lax.psum(jnp.sum(inputs_f32 * inputs_f32, axis=1, keepdims=True), 'tp')  15.2 us
    ppermute x3, waiting for transfers between devices, targets_tell(): piece_next = lax.ppermute(piece_next, axis_name='sp', perm=next_value)  9.4 us
    all_gather x1, blocking collectives, body(): lax.all_gather(latent_proj.astype(jnp.bfloat16), 'tp', axis=1, tiled=True)  9.26 us
    unnamed x33, local copies, waits for them, and re-layouts  7.88 us
    ppermute x3, starting transfers between devices, targets_tell(): piece_next = lax.ppermute(piece_next, axis_name='sp', perm=next_value)  4.24 us
    dot_general x1, matrix products, body(): jnp.dot(conv_mixed, output_conv, preferred_element_type=jnp.float32)  3.21 us
  transfers between devices with their start and end apart: 7, of which 4 were waited for; matrix products, arithmetic and copies ran while one was open for 9% of the time, Pallas kernels for 0%

profile of v1, /device:TPU:0, one launch (start us, length us, event | category | flops | bytes accessed | tf_op | source)
XLA Modules:
  0.0 130.5 jit_solution(1879229346890879437)
XLA Ops:
  7.3 0.7 all-gather.2.cloned.1.call-update
  8.0 1.0 multiply_reduce_fusion
  9.1 1.2 copy.19
  10.3 1.3 copy.20
  11.6 1.2 copy.21
  12.8 15.2 %psum.7 = f32[256,1]{0,1:T(1,128)S(1)} all-reduce(f32[256,1]{0,1:T(1,128)S(1)} %bitcast.74), channel_id=1, replica_groups=mesh['sp'=4,'tp'=8] {'tp'}, use_global_device_ids=true, to_apply=%region_1.0 | all-reduce | flops 256 | bytes 2048 | tf_op jit(solution)/shard_map/psum | solution.py:96
  28.0 0.5 slice_bitcast_fusion.13
  28.6 0.9 constant_dynamic-update-slice_fusion.5
  29.5 0.7 constant_dynamic-update-slice_fusion.4
  30.3 0.7 constant_dynamic-update-slice_fusion.3
  31.0 0.8 constant_dynamic-update-slice_fusion.2
  31.8 0.8 constant_dynamic-update-slice_fusion.1
  32.7 0.8 constant_dynamic-update-slice_fusion
  33.5 2.7 %all-gather.2.cloned.1.call-done = bf16[256,2048]{1,0:T(8,128)(2,1)} async-done(((bf16[256,256]{1,0:T(8,128)(2,1)}), bf16[256,2048]{1,0:T(8,128)(2,1)}) %all-gather.2.cloned.1.call-update) | async-done | bytes 1048592 | tf_op jit(solution)/shard_map/all_gather | solution.py:98
  36.2 3.1 %convolution_multiply_fusion = f32[256,704]{0,1:T(8,128)S(1)} fusion(bf16[2048,704]{0,1:T(8,128)(2,1)} %constant_dynamic-update-slice_fusion, bf16[256,2048]{1,0:T(8,128)(2,1)} %all-gather.2.cloned.1.call-done, f32[2048]{0:T(1024)S(1)} %copy-done.7, f32[256]{0:T(256)S(1)} %bitcast.75), kind=kOutput, calls=%fused_computation.6 | convolution fusion | flops 739950592 | bytes 4662272 | tf_op jit(solution)/shard_map/dot_general | solution.py:100
  39.7 0.2 fusion.52
  39.9 1.5 %collective-permute-start = (bf16[256,64]{0,1:T(8,128)(2,1)S(1)}, bf16[256,64]{0,1:T(8,128)(2,1)S(1)}, u32[]{:S(2)}, u32[]{:S(2)}) collective-permute-start(bf16[256,64]{0,1:T(8,128)(2,1)S(1)} %maximum_bitcast_fusion), channel_id=1, source_target_pairs={{0,8},{8,16},{16,24},{24,0},{1,9},{9,17},{17,25},{25,1},{2,10},{10... | collective-permute-start | bytes 98312 | tf_op jit(solution)/shard_map/ppermute | solution.py:23
  41.6 9.3 %all_gather.10 = bf16[256,512]{0,1:T(8,128)(2,1)S(1)} all-gather(bf16[256,64]{0,1:T(8,128)(2,1)S(1)} %slice.196), channel_id=1, replica_groups=mesh['sp'=4,'tp'=8] {'tp'}, dimensions={1}, use_global_device_ids=true | all-gather | bytes 294912 | tf_op jit(solution)/shard_map/all_gather | solution.py:122
  51.1 0.4 convolution_convert_fusion
  51.5 15.8 %all_gather.11 = bf16[1024,256]{1,0:T(8,128)(2,1)S(1)} all-gather(bf16[256,256]{1,0:T(8,128)(2,1)S(1)} %convolution_convert_fusion), channel_id=1, replica_groups=mesh['sp'=4,'tp'=8] {'sp'}, dimensions={0}, use_global_device_ids=true | all-gather | bytes 655360 | tf_op jit(solution)/shard_map/all_gather | solution.py:139
  67.3 2.7 %collective-permute-start.3 = (bf16[1,128]{0,1:T(8,128)(2,1)S(1)}, bf16[1,128]{0,1:T(8,128)(2,1)S(1)}, u32[]{:S(2)}, u32[]{:S(2)}) collective-permute-start(bf16[1,128]{0,1:T(8,128)(2,1)S(1)} %get-tuple-element.26), channel_id=1, source_target_pairs={{0,8},{8,16},{16,24},{1,9},{9,17},{17,25},{2,10},{10,18},{18,26},{... | collective-permute-start | bytes 776 | tf_op jit(solution)/shard_map/ppermute | solution.py:37
  70.0 1.3 collective-permute-start.4
  71.3 2.7 %collective-permute-start.1 = (bf16[256,64]{0,1:T(8,128)(2,1)S(1)}, bf16[256,64]{0,1:T(8,128)(2,1)S(1)}, u32[]{:S(2)}, u32[]{:S(2)}) collective-permute-start(bf16[256,64]{0,1:T(8,128)(2,1)S(1)} %collective-permute-done), channel_id=1, source_target_pairs={{0,8},{8,16},{16,24},{24,0},{1,9},{9,17},{17,25},{25,1},{2,10},{10... | collective-permute-start | bytes 98312 | tf_op jit(solution)/shard_map/ppermute | solution.py:23
  74.0 0.3 convolution_bitcast_fusion.1
  74.3 3.8 %collective-permute-done.1 = bf16[256,64]{0,1:T(8,128)(2,1)S(1)} collective-permute-done((bf16[256,64]{0,1:T(8,128)(2,1)S(1)}, bf16[256,64]{0,1:T(8,128)(2,1)S(1)}, u32[]{:S(2)}, u32[]{:S(2)}) %collective-permute-start.1) | collective-permute-done | bytes 32800 | tf_op jit(solution)/shard_map/ppermute | solution.py:23
  78.2 5.6 %collective-permute-done.2 = bf16[256,64]{0,1:T(8,128)(2,1)S(1)} collective-permute-done((bf16[256,64]{0,1:T(8,128)(2,1)S(1)}, bf16[256,64]{0,1:T(8,128)(2,1)S(1)}, u32[]{:S(2)}, u32[]{:S(2)}) %collective-permute-start.2) | collective-permute-done | bytes 32800 | tf_op jit(solution)/shard_map/ppermute | solution.py:23
  83.9 0.4 fusion.67
  84.3 0.3 fusion.7
  84.7 2.4 %fusion.9 = f32[256,2048]{1,0:T(8,128)} fusion(bf16[128,2048]{1,0:T(8,128)(2,1)S(1)} %copy-done, f32[1,256,1024]{2,1,0:T(8,128)S(1)} %get-tuple-element.44, f32[256]{0:T(256)S(1)} %get-tuple-element.43, bf16[1024,1,256]{2,0,1:T(8,128)(2,1)S(1)} %bitcast.71, f32[256]{0:T(256)S(1)} %get-tuple-element.42, f32[256]{0:T(256)S(1)} %get-tuple-element.41), kind=kOutput, calls=%fused_computation.19 | convolution fusion | flops 201949184 | bytes 3935232 | tf_op jit(solution)/shard_map/dot_general | solution.py:178
  87.1 3.2 %fusion = bf16[256,2048]{1,0:T(8,128)(2,1)} fusion(f32[256,2048]{1,0:T(8,128)} %fusion.9, bf16[128,2048]{1,0:T(8,128)(2,1)S(1)} %copy-done.2, f32[258,128]{0,1:T(8,128)S(1)} %maximum_convert_fusion, f32[256,704]{0,1:T(8,128)S(1)} %convolution_multiply_fusion, f32[128]{0:T(128)} %get-tuple-element.38, f32[128]{0:T(128)} %get-tuple-element.39, ...), kind=kOutput, calls=%fused_computation.1 | convolution fusion | flops 135495680 | bytes 4195840 | tf_op jit(solution)/shard_map/dot_general | solution.py:179
  90.3 0.6 log_add_fusion
  90.9 32.8 %reduce-scatter.2.cloned.1.call-done = bf16[32,2048]{1,0:T(8,128)(2,1)} async-done(((bf16[256,2048]{1,0:T(8,128)(2,1)}), bf16[32,2048]{1,0:T(8,128)(2,1)}) %reduce-scatter.2.cloned.1.call-update) | async-done | bytes 131088 | tf_op jit(solution)/shard_map/reduce_scatter | solution.py:176
  (52 shorter events, 1.0 us)
Async XLA Ops:
  7.2 77.5 %copy-start = (bf16[128,2048]{1,0:T(8,128)(2,1)S(1)}, bf16[128,2048]{1,0:T(8,128)(2,1)}, u32[]{:S(2)}) copy-start(bf16[128,2048]{1,0:T(8,128)(2,1)} %param.24) | copy-start | bytes 1572868
  7.2 20.8 %copy-start.5 = (bf16[3,128]{1,0:T(4,128)(2,1)S(1)}, bf16[3,128]{1,0:T(4,128)(2,1)}, u32[]{:S(2)}) copy-start(bf16[3,128]{1,0:T(4,128)(2,1)} %param.23) | copy-start | bytes 2308
  7.2 21.4 %copy-start.1 = (bf16[2048,192]{0,1:T(8,128)(2,1)S(1)}, bf16[2048,192]{0,1:T(8,128)(2,1)}, u32[]{:S(2)}) copy-start(bf16[2048,192]{0,1:T(8,128)(2,1)} %param.15) | copy-start | bytes 2359300
  7.2 22.3 %copy-start.3 = (bf16[2048,64]{0,1:T(8,128)(2,1)S(1)}, bf16[2048,64]{0,1:T(8,128)(2,1)}, u32[]{:S(2)}) copy-start(bf16[2048,64]{0,1:T(8,128)(2,1)} %param.16) | copy-start | bytes 786436
  7.2 23.0 %copy-start.4 = (bf16[2048,64]{0,1:T(8,128)(2,1)S(1)}, bf16[2048,64]{0,1:T(8,128)(2,1)}, u32[]{:S(2)}) copy-start(bf16[2048,64]{0,1:T(8,128)(2,1)} %param.17) | copy-start | bytes 786436
  7.2 29.0 %all-gather.2.cloned.1.call-start = ((), (), s32[]{:S(2)}) async-start(), calls=%async_computation.1 | async-start | bytes 1179648 | tf_op jit(solution)/shard_map/all_gather | solution.py:98
  8.0 115.7 %reduce-scatter.2.cloned.1.call-start = ((), (), s32[]{:S(2)}) async-start(), calls=%async_computation.2 | async-start | bytes 1179648 | tf_op jit(solution)/shard_map/reduce_scatter | solution.py:176
  28.6 7.6 %copy-start.7 = (f32[2048]{0:T(1024)S(1)}, f32[2048]{0:T(1024)}, u32[]{:S(2)}) copy-start(f32[2048]{0:T(1024)} %param.14) | copy-start | bytes 24580
  36.2 14.9 %copy-start.6 = (bf16[512,256]{1,0:T(8,128)(2,1)S(1)}, bf16[512,256]{1,0:T(8,128)(2,1)}, u32[]{:S(2)}) copy-start(bf16[512,256]{1,0:T(8,128)(2,1)} %param.19) | copy-start | bytes 786436
  36.2 14.9 %copy-start.8 = (f32[512]{0:T(512)S(1)}, f32[512]{0:T(512)}, u32[]{:S(2)}) copy-start(f32[512]{0:T(512)} %param.18) | copy-start | bytes 6148
  39.9 31.4 %collective-permute-start = (bf16[256,64]{0,1:T(8,128)(2,1)S(1)}, bf16[256,64]{0,1:T(8,128)(2,1)S(1)}, u32[]{:S(2)}, u32[]{:S(2)}) collective-permute-start(bf16[256,64]{0,1:T(8,128)(2,1)S(1)} %maximum_bitcast_fusion), channel_id=1, source_target_pairs={{0,8},{8,16},{16,24},{24,0},{1,9},{9,17},{17,25},{25,1},{2,10},{10... | collective-permute-start | bytes 98312 | tf_op jit(solution)/shard_map/ppermute | solution.py:23
  67.3 10.9 %collective-permute-start.3 = (bf16[1,128]{0,1:T(8,128)(2,1)S(1)}, bf16[1,128]{0,1:T(8,128)(2,1)S(1)}, u32[]{:S(2)}, u32[]{:S(2)}) collective-permute-start(bf16[1,128]{0,1:T(8,128)(2,1)S(1)} %get-tuple-element.26), channel_id=1, source_target_pairs={{0,8},{8,16},{16,24},{1,9},{9,17},{17,25},{2,10},{10,18},{18,26},{... | collective-permute-start | bytes 776 | tf_op jit(solution)/shard_map/ppermute | solution.py:37
  70.0 8.1 %collective-permute-start.4 = (bf16[1,128]{0,1:T(8,128)(2,1)S(1)}, bf16[1,128]{0,1:T(8,128)(2,1)S(1)}, u32[]{:S(2)}, u32[]{:S(2)}) collective-permute-start(bf16[1,128]{0,1:T(8,128)(2,1)S(1)} %get-tuple-element.36), channel_id=1, source_target_pairs={{8,0},{16,8},{24,16},{9,1},{17,9},{25,17},{10,2},{18,10},{26,18},{... | collective-permute-start | bytes 776 | tf_op jit(solution)/shard_map/ppermute | solution.py:38
  71.3 6.8 %collective-permute-start.1 = (bf16[256,64]{0,1:T(8,128)(2,1)S(1)}, bf16[256,64]{0,1:T(8,128)(2,1)S(1)}, u32[]{:S(2)}, u32[]{:S(2)}) collective-permute-start(bf16[256,64]{0,1:T(8,128)(2,1)S(1)} %collective-permute-done), channel_id=1, source_target_pairs={{0,8},{8,16},{16,24},{24,0},{1,9},{9,17},{17,25},{25,1},{2,10},{10... | collective-permute-start | bytes 98312 | tf_op jit(solution)/shard_map/ppermute | solution.py:23
  78.1 5.7 %collective-permute-start.2 = (bf16[256,64]{0,1:T(8,128)(2,1)S(1)}, bf16[256,64]{0,1:T(8,128)(2,1)S(1)}, u32[]{:S(2)}, u32[]{:S(2)}) collective-permute-start(bf16[256,64]{0,1:T(8,128)(2,1)S(1)} %collective-permute-done.1), channel_id=1, source_target_pairs={{0,8},{8,16},{16,24},{24,0},{1,9},{9,17},{17,25},{25,1},{2,10},{10... | collective-permute-start | bytes 98312 | tf_op jit(solution)/shard_map/ppermute | solution.py:23
  84.3 2.8 %copy-start.2 = (bf16[128,2048]{1,0:T(8,128)(2,1)S(1)}, bf16[128,2048]{1,0:T(8,128)(2,1)}, u32[]{:S(2)}) copy-start(bf16[128,2048]{1,0:T(8,128)(2,1)} %param.25) | copy-start | bytes 1572868
Sparse Core Ops, SparseCore 0:
  9.9 26.2 all-gather.1
  90.5 33.1 reduce-scatter.1
